TPU v7x, 32 devices: a whole 2x2x4 slice. The times are simulated.
32 devices in a mesh: ep: 16 (over z, y, x), tp: 2 (over core).
Axes of the slice: x: 2, y: 2, z: 4, core: 2. Of those that a mesh axis runs over, the one named last changes fastest.
Arguments:
- tokens: bfloat16 [16, 2048], P('ep'), may hold values from -6 to 6
- norm_gain: float32 [2048], replicated, may hold values from 0.1 to 1.9
- w_query: bfloat16 [2048, 512], P('ep', 'tp'), may hold values from -0.125 to 0.125
- w_key: bfloat16 [2048, 512], P('ep', 'tp'), may hold values from -0.125 to 0.125
- w_value: bfloat16 [2048, 1024], P('ep', 'tp'), may hold values from -0.125 to 0.125
- w_outgate: bfloat16 [2048, 1024], P('ep', 'tp'), may hold values from -0.125 to 0.125
- decay_in: bfloat16 [2048, 16], replicated, may hold values from -0.125 to 0.125
- decay_out: bfloat16 [16, 512], P(None, 'tp'), may hold values from -1.5 to 1.5
- decay_bias: float32 [512], P('tp'), may hold values from -40 to 4
- gla_state: float32 [16, 2, 256, 512], P('ep', 'tp'), may hold values from -6 to 6
- head_gain: float32 [512], replicated, may hold values from 0.1 to 1.9
- w_output: bfloat16 [1024, 2048], P(None, 'ep'), may hold values from -0.1875 to 0.1875
- moe_gain: float32 [2048], replicated, may hold values from 0.1 to 1.9
- expert_ids: int32 [16, 6], replicated, may hold values from 0 to 15, all different within a row; in each aligned block of 16 rows (0 to 15, 16 to 31, ...) at most 12 rows name the same one
- route_weight: float32 [16, 6], replicated, may hold values from 0.2 to 1
- expert_gate: bfloat16 [16, 2048, 512], P('ep', None, 'tp'), may hold values from -0.125 to 0.125
- expert_up: bfloat16 [16, 2048, 512], P('ep', None, 'tp'), may hold values from -0.125 to 0.125
- expert_down: bfloat16 [16, 512, 2048], P('ep', 'tp'), may hold values from -0.25 to 0.25
- shared_gate: bfloat16 [2048, 512], P(None, 'tp'), may hold values from -0.125 to 0.125
- shared_up: bfloat16 [2048, 512], P(None, 'tp'), may hold values from -0.125 to 0.125
- shared_down: bfloat16 [512, 2048], P('tp'), may hold values from -0.25 to 0.25
Outputs:
- result: bfloat16 [16, 2048], P(None, 'ep')
- new_state: float32 [16, 2, 256, 512], P('ep', 'tp')
Inputs may be any that keep to these rules, and one draw needn't show every extreme that they name: `expert_ids`: each row names 6 different experts. No expert is named by more than 12 rows in all, a bound that some block reaches.
All inputs are finite; a program needn't handle non-finite values.
Results may differ from a plain program's by a relative error of at most 0.018.
Values may be sent and summed in bfloat16 or wider, within the bound.
A program may use at most 64 MiB of HBM per device.

v0:
```python
import jax
import jax.numpy as jnp
from jax import lax
from jax.sharding import PartitionSpec as P

DK = 256
DV = 512


EPSILON = 1e-06
DECAY_TEMPER = 16.0


def rms_scale(values):
    return lax.rsqrt(jnp.mean(values * values, axis=-1, keepdims=True) + EPSILON)


def slot_positions(expert_ids, expert_count):
    flat_ids = expert_ids.reshape(-1)
    onehot = (flat_ids[:, None] == jnp.arange(expert_count, dtype=jnp.int32)[None, :]).astype(
        jnp.int32
    )
    before = jnp.cumsum(onehot, axis=0) - onehot
    position = jnp.sum(before * onehot, axis=1)
    return (flat_ids, position)


def expert_block(rows, moe_gain, gate_weight, up_weight, down_weight):
    row_float = rows.astype(jnp.float32)
    normal_rows = (row_float * rms_scale(row_float) * moe_gain).astype(jnp.bfloat16)
    gate_values = jnp.einsum(
        "ecd,edf->ecf", normal_rows, gate_weight, preferred_element_type=jnp.float32
    )
    upward = jnp.einsum("ecd,edf->ecf", normal_rows, up_weight, preferred_element_type=jnp.float32)
    active = (jax.nn.silu(gate_values) * upward).astype(jnp.bfloat16)
    return jnp.einsum(
        "ecf,efd->ecd", active, down_weight, preferred_element_type=jnp.float32
    ).astype(jnp.bfloat16)


def per_device(
    tokens,
    norm_gain,
    w_query,
    w_key,
    w_value,
    w_outgate,
    decay_in,
    decay_out,
    decay_bias,
    gla_state,
    head_gain,
    w_output,
    moe_gain,
    expert_ids,
    route_weight,
    expert_gate,
    expert_up,
    expert_down,
    shared_gate,
    shared_up,
    shared_down,
):
    ep_size = lax.axis_size("ep")
    tp_size = lax.axis_size("tp")
    seq_dev = tokens.shape[0]
    top_count = expert_ids.shape[1]
    exp_dev = expert_gate.shape[0]
    experts = exp_dev * ep_size
    all_rows = seq_dev * ep_size
    capacity = 2 * seq_dev * top_count // exp_dev
    heads_local = w_query.shape[1] // DK
    tok_float = tokens.astype(jnp.float32)
    normed = (tok_float * rms_scale(tok_float) * norm_gain).astype(jnp.bfloat16)
    span_sizes = (w_query.shape[1], w_key.shape[1], w_value.shape[1], w_outgate.shape[1])
    raw_columns, normed_columns = (
        lax.all_to_all(tokens, "ep", split_axis=1, concat_axis=0, tiled=True),
        lax.all_to_all(normed, "ep", split_axis=1, concat_axis=0, tiled=True),
    )
    joined = lax.psum_scatter(
        jnp.concatenate(
            [
                jnp.dot(normed_columns, weight, preferred_element_type=jnp.float32)
                for weight in (w_query, w_key, w_value, w_outgate)
            ],
            axis=1,
        ),
        "ep",
        scatter_dimension=0,
        tiled=True,
    )
    column_edges = [
        0,
        span_sizes[0],
        span_sizes[0] + span_sizes[1],
        span_sizes[0] + span_sizes[1] + span_sizes[2],
        sum(span_sizes),
    ]
    projected = tuple(
        (joined[:, column_edges[number] : column_edges[number + 1]] for number in range(4))
    )
    query_rows, key_rows, value_rows, gate_rows = (
        part_sum.astype(jnp.bfloat16) for part_sum in projected
    )
    decay_low = jnp.dot(normed, decay_in, preferred_element_type=jnp.float32).astype(jnp.bfloat16)
    decay_pre = jnp.dot(decay_low, decay_out, preferred_element_type=jnp.float32) + decay_bias
    decay_rate = jnp.exp(jax.nn.log_sigmoid(decay_pre) / DECAY_TEMPER).reshape(
        seq_dev, heads_local, DK
    )
    query_heads = query_rows.astype(jnp.float32).reshape(seq_dev, heads_local, DK) * DK ** (-0.5)
    key_heads = key_rows.astype(jnp.float32).reshape(seq_dev, heads_local, DK)
    value_heads = value_rows.astype(jnp.float32).reshape(seq_dev, heads_local, DV)
    new_state = (
        decay_rate[..., None] * gla_state + key_heads[..., None] * value_heads[:, :, None, :]
    )
    read_out = jnp.einsum("shk,shkv->shv", query_heads, new_state, precision=lax.Precision.HIGHEST)
    gate_heads = gate_rows.astype(jnp.float32).reshape(seq_dev, heads_local, DV)
    mixed_heads = (read_out * rms_scale(read_out) * head_gain * jax.nn.silu(gate_heads)).astype(
        jnp.bfloat16
    )
    head_weights = w_output.reshape(tp_size, heads_local * DV, w_output.shape[1])
    shard_rows = lax.all_gather(mixed_heads, ("ep", "tp"), axis=0, tiled=True)
    owners = lax.iota(jnp.int32, shard_rows.shape[0])
    select = (owners[:, None] % tp_size == lax.iota(jnp.int32, tp_size)[None, :]).astype(
        jnp.bfloat16
    )
    chosen = jnp.einsum(
        "mt,tcd->mcd", select, head_weights, preferred_element_type=jnp.float32
    ).astype(jnp.bfloat16)
    spread = jnp.einsum("msc,mcd->msd", shard_rows, chosen, preferred_element_type=jnp.float32)
    attention = (
        spread.reshape(ep_size, tp_size, seq_dev, -1)
        .sum(axis=1)
        .reshape(all_rows, -1)
        .astype(jnp.bfloat16)
    )
    hidden = (raw_columns.astype(jnp.float32) + attention.astype(jnp.float32)).astype(jnp.bfloat16)
    flat_ids, position = slot_positions(expert_ids, experts)
    owner_rows = lax.iota(jnp.int32, all_rows * top_count) // top_count
    slot_table = (
        jnp.full((experts, capacity), all_rows, jnp.int32).at[flat_ids, position].set(owner_rows)
    )
    padded = jnp.concatenate([hidden, jnp.zeros((1, hidden.shape[1]), jnp.bfloat16)], axis=0)
    routed_rows, shared_rows = (
        lax.all_to_all(padded[slot_table], "ep", split_axis=0, concat_axis=2, tiled=True),
        lax.all_to_all(
            hidden.reshape(ep_size, seq_dev, hidden.shape[1]),
            "ep",
            split_axis=0,
            concat_axis=2,
            tiled=True,
        ),
    )
    routed_part = expert_block(routed_rows, moe_gain, expert_gate, expert_up, expert_down)
    shared_part = expert_block(
        shared_rows, moe_gain, shared_gate[None], shared_up[None], shared_down[None]
    )
    routed_sum, shared_sum = (
        lax.psum(routed_part, "tp").astype(jnp.float32),
        lax.psum(shared_part, "tp").astype(jnp.float32),
    )
    routed_out = routed_sum.astype(jnp.bfloat16)
    shared_out = shared_sum.astype(jnp.bfloat16)
    back_routed, back_shared = (
        lax.all_to_all(routed_out, "ep", split_axis=2, concat_axis=0, tiled=True),
        lax.all_to_all(shared_out, "ep", split_axis=2, concat_axis=0, tiled=True),
    )
    picked = back_routed.reshape(experts * capacity, -1)[flat_ids * capacity + position]
    weighted = picked.astype(jnp.float32).reshape(all_rows, top_count, -1) * route_weight[..., None]
    moe_columns = jnp.sum(weighted, axis=1) + back_shared.reshape(all_rows, -1).astype(jnp.float32)
    result = (hidden.astype(jnp.float32) + moe_columns).astype(jnp.bfloat16)
    return (result, new_state)


def solution(mesh):
    return jax.shard_map(
        per_device,
        mesh=mesh,
        in_specs=(
            P("ep", None),
            P(),
            P("ep", "tp"),
            P("ep", "tp"),
            P("ep", "tp"),
            P("ep", "tp"),
            P(),
            P(None, "tp"),
            P("tp"),
            P("ep", "tp", None, None),
            P(),
            P(None, "ep"),
            P(),
            P(),
            P(),
            P("ep", None, "tp"),
            P("ep", None, "tp"),
            P("ep", "tp", None),
            P(None, "tp"),
            P(None, "tp"),
            P("tp", None),
        ),
        out_specs=(P(None, "ep"), P("ep", "tp", None, None)),
        check_vma=False,
    )
```

profile of v0, /device:TPU:0, one launch (start us, length us, event | category | flops | bytes accessed | tf_op | source)
XLA Modules:
  0.0 244.8 jit_solution(1949194534503189319)
XLA Ops:
  0.6 0.0 copy-start
  0.6 0.0 copy-start.11
  0.7 1.4 multiply_reduce_fusion.2
  2.8 1.3 convert_bitcast_fusion.3
  4.1 8.3 %all-to-all-start.1 = ((bf16[1,16,128]{2,0,1:T(2,128)(2,1)}), bf16[1,16,128]{2,0,1:T(2,128)(2,1)S(1)}, u32[]{:S(2)}, u32[]{:S(2)}) async-start(bf16[1,16,128]{2,0,1:T(2,128)(2,1)} %convert_bitcast_fusion.3), calls=%async_computation.1 | async-start | bytes 16384 | tf_op jit(solution)/shard_map/all_to_all | solution.py:78
  12.5 0.8 copy.66
  13.3 0.1 eq.33
  13.4 0.1 reshape.455
  13.5 0.1 fusion.20
  13.5 0.0 copy-start.10
  13.6 0.1 reduce_window_sum.11
  13.7 0.2 select_reduce_fusion
  13.9 5.4 %scatter_fusion = s32[16,12]{1,0:T(8,128)S(1)} fusion(s32[16,12]{1,0:T(8,128)S(1)} %broadcast_in_dim.7, s32[96]{0:T(128)S(1)} %get-tuple-element.7, s32[96]{0:T(128)S(1)} %and_select_fusion), kind=kCustom, calls=%fused_computation.2 | custom fusion | bytes 1920 | tf_op jit(solution)/shard_map/scatter | solution.py:141
  19.3 0.1 reshape.472
  19.4 1.1 fusion.11
  20.5 0.7 fusion.51
  21.2 4.2 %convolution_convert_fusion = bf16[32,512,128]{2,0,1:T(8,128)(2,1)} fusion(bf16[2,512,128]{2,1,0:T(8,128)(2,1)} %bitcast.143, s32[32]{0:T(128)S(1)} %and_select_fusion.1), kind=kOutput, calls=%fused_computation.5 | convolution fusion | flops 10485824 | bytes 4456576 | tf_op jit(solution)/shard_map/mt,tcd->mcd/dot_general | solution.py:127
  25.5 0.6 dynamic-slice
  26.1 6.9 %all-to-all-start = ((bf16[1,16,128]{2,0,1:T(2,128)(2,1)}), bf16[1,16,128]{2,0,1:T(2,128)(2,1)S(1)}, u32[]{:S(2)}, u32[]{:S(2)}) async-start(bf16[1,16,128]{2,0,1:T(2,128)(2,1)} %bitcast), calls=%async_computation | async-start | bytes 16384 | tf_op jit(solution)/shard_map/all_to_all | solution.py:77
  33.0 0.1 fusion.36
  33.1 0.1 fusion.38
  33.3 0.1 fusion.40
  33.4 0.1 fusion.42
  33.5 78.2 %all-reduce.1 = bf16[16,1536]{1,0:T(8,128)(2,1)S(1)} all-reduce(f32[16,1536]{1,0:T(8,128)S(1)} %pad_maximum_fusion), channel_id=3, replica_groups=mesh['ep'=16,'tp'=2] {'ep'}, use_global_device_ids=true, to_apply=%region_1.0.clone | all-reduce | flops 24576 | bytes 147456
  111.7 0.7 dynamic-slice_convert_fusion
  112.4 1.2 multiply_add_fusion
  113.6 0.0 copy-start.1
  113.6 0.8 copy-done.1
  114.4 0.4 fusion.12
  114.8 0.6 multiply_reduce_fusion.3
  116.1 36.5 %all-gather.1 = bf16[32,1,512]{2,1,0:T(2,128)(2,1)S(1)} all-gather(bf16[1,1,512]{2,1,0:T(2,128)(2,1)S(1)} %reshape.496), channel_id=2, replica_groups=mesh['ep'=16,'tp'=2] {'ep','tp'}, dimensions={0}, use_global_device_ids=true | all-gather | bytes 33792 | tf_op jit(solution)/shard_map/all_gather | solution.py:122
  152.6 6.4 %fusion = f32[32,1,128]{2,1,0:T(1,128)S(1)} fusion(bf16[32,512,128]{2,0,1:T(8,128)(2,1)} %convolution_convert_fusion, bf16[32,1,512]{2,1,0:T(2,128)(2,1)S(1)} %all-gather.1), kind=kOutput, calls=%fused_computation.3 | convolution fusion | flops 4194304 | bytes 4243456 | tf_op jit(solution)/shard_map/msc,mcd->msd/dot_general | solution.py:130
  159.1 0.0 all-to-all-done
  159.1 0.6 copy.73
  159.7 3.4 %all-to-all-start.4 = ((bf16[16,1,128]{2,1,0:T(2,128)(2,1)}), bf16[16,1,128]{2,1,0:T(2,128)(2,1)S(1)}, u32[]{:S(2)}, u32[]{:S(2)}) async-start(bf16[16,1,128]{2,1,0:T(2,128)(2,1)} %copy.73), calls=%async_computation.4 | async-start | bytes 16384 | tf_op jit(solution)/shard_map/all_to_all | solution.py:146
  163.2 0.8 gather_fusion
  163.9 0.6 reshape.471
  164.6 5.8 %all-to-all-done.4 = bf16[16,1,128]{2,1,0:T(2,128)(2,1)S(1)} async-done(((bf16[16,1,128]{2,1,0:T(2,128)(2,1)}), bf16[16,1,128]{2,1,0:T(2,128)(2,1)S(1)}, u32[]{:S(2)}, u32[]{:S(2)}) %all-to-all-start.4) | async-done | bytes 4128 | tf_op jit(solution)/shard_map/all_to_all | solution.py:146
  170.4 3.5 %all-to-all-start.2 = ((bf16[16,12,128]{2,1,0:T(8,128)(2,1)}), bf16[16,12,128]{2,1,0:T(8,128)(2,1)S(1)}, u32[]{:S(2)}, u32[]{:S(2)}) async-start(bf16[16,12,128]{2,1,0:T(8,128)(2,1)} %reshape.471), calls=%async_computation.2 | async-start | bytes 131072 | tf_op jit(solution)/shard_map/all_to_all | solution.py:145
  173.9 0.6 multiply_reduce_fusion.1
  175.3 0.2 fusion.64
  175.5 0.3 fusion.65
  175.8 1.5 fusion.66
  177.3 4.1 %all-to-all-done.2 = bf16[16,12,128]{2,1,0:T(8,128)(2,1)S(1)} async-done(((bf16[16,12,128]{2,1,0:T(8,128)(2,1)}), bf16[16,12,128]{2,1,0:T(8,128)(2,1)S(1)}, u32[]{:S(2)}, u32[]{:S(2)}) %all-to-all-start.2) | async-done | bytes 49184 | tf_op jit(solution)/shard_map/all_to_all | solution.py:145
  181.4 0.1 fusion.15
  181.5 0.1 fusion.18
  181.7 1.5 fusion.9
  183.2 2.0 fusion.2
  185.1 3.6 %all-reduce.2 = (bf16[1,12,2048]{2,1,0:T(8,128)(2,1)S(1)}, bf16[1,1,2048]{2,1,0:T(2,128)(2,1)S(1)}) all-reduce(bf16[1,12,2048]{2,1,0:T(8,128)(2,1)S(1)} %fusion.2, bf16[1,1,2048]{2,1,0:T(2,128)(2,1)S(1)} %convert_element_type.218), channel_id=1, replica_groups=mesh['ep'=16,'tp'=2] {'tp'}, use_global_device_ids=true, to_apply=%region_8.9 | all-reduce | flops 26624 | bytes 106496 | tf_op jit(solution)/shard_map/psum | solution.py:159
  188.7 2.1 copy.74
  190.8 3.8 %all-to-all-start.5 = ((bf16[1,1,2048]{1,0,2:T(2,128)(2,1)}), bf16[1,1,2048]{1,0,2:T(2,128)(2,1)S(1)}, u32[]{:S(2)}, u32[]{:S(2)}) async-start(bf16[1,1,2048]{1,0,2:T(2,128)(2,1)} %copy.74), calls=%async_computation.5 | async-start | bytes 2097152 | tf_op jit(solution)/shard_map/all_to_all | solution.py:166
  194.6 0.1 copy.72
  194.7 0.8 copy.69
  195.6 0.5 broadcast.257
  196.1 12.4 %reduce.11 = bf16[2048,12]{1,0:T(8,128)(2,1)} reduce(bf16[2048,1,12]{2,1,0:T(2,128)(2,1)S(1)} %bitcast.139, bf16[]{:T(256)} %broadcast.257), dimensions={1}, to_apply=%bitcast.122.reduce_sub_computation | reduce | bytes 98306
  208.4 2.4 reshape.519
  210.9 8.5 %all-to-all-done.5 = bf16[1,1,2048]{1,0,2:T(2,128)(2,1)S(1)} async-done(((bf16[1,1,2048]{1,0,2:T(2,128)(2,1)}), bf16[1,1,2048]{1,0,2:T(2,128)(2,1)S(1)}, u32[]{:S(2)}, u32[]{:S(2)}) %all-to-all-start.5) | async-done | bytes 4128 | tf_op jit(solution)/shard_map/all_to_all | solution.py:166
  219.3 6.8 %all-to-all-start.3 = ((bf16[16,2,768]{2,1,0:T(2,128)(2,1)}), bf16[16,2,768]{2,1,0:T(2,128)(2,1)S(1)}, u32[]{:S(2)}, u32[]{:S(2)}) async-start(bf16[16,2,768]{2,1,0:T(2,128)(2,1)} %reshape.519), calls=%async_computation.3 | async-start | bytes 98304 | tf_op jit(solution)/shard_map/all_to_all | solution.py:165
  226.1 15.2 %convert_reduce_fusion = f32[2048]{0:T(1024)S(1)} fusion(bf16[1,1,2048]{1,0,2:T(2,128)(2,1)S(1)} %all-to-all-done.5), kind=kLoop, calls=%fused_computation.17 | loop fusion | flops 2048 | bytes 12288 | tf_op jit(solution)/shard_map/convert_element_type | solution.py:170
  241.3 1.4 reshape.520
  242.8 0.6 copy.70
  243.4 0.7 gather_fusion.1
  244.1 0.1 multiply_reduce_fusion
  244.2 0.6 fusion.30
  (54 shorter events, 0.3 us)
Async XLA Ops:
  0.6 182.6 %copy-start = (bf16[1,256,2048]{2,1,0:T(8,128)(2,1)S(1)}, bf16[1,256,2048]{2,1,0:T(8,128)(2,1)}, u32[]{:S(2)}) copy-start(bf16[1,256,2048]{2,1,0:T(8,128)(2,1)} %param.38) | copy-start | bytes 3145732
  0.6 24.8 %copy-start.11 = (u32[32]{0:T(128)S(1)}, u32[32]{0:T(128)}, u32[]{:S(2)}) copy-start(u32[32]{0:T(128)} %constant.104) | copy-start | bytes 388
  0.7 32.3 %copy-start.4 = (bf16[128,512]{1,0:T(8,128)(2,1)S(1)}, bf16[128,512]{1,0:T(8,128)(2,1)}, u32[]{:S(2)}) copy-start(bf16[128,512]{1,0:T(8,128)(2,1)} %param.26) | copy-start | bytes 393220
  0.7 32.4 %copy-start.5 = (bf16[128,512]{1,0:T(8,128)(2,1)S(1)}, bf16[128,512]{1,0:T(8,128)(2,1)}, u32[]{:S(2)}) copy-start(bf16[128,512]{1,0:T(8,128)(2,1)} %param.25) | copy-start | bytes 393220
  0.7 32.6 %copy-start.6 = (bf16[128,256]{1,0:T(8,128)(2,1)S(1)}, bf16[128,256]{1,0:T(8,128)(2,1)}, u32[]{:S(2)}) copy-start(bf16[128,256]{1,0:T(8,128)(2,1)} %param.24) | copy-start | bytes 196612
  0.7 32.7 %copy-start.7 = (bf16[128,256]{1,0:T(8,128)(2,1)S(1)}, bf16[128,256]{1,0:T(8,128)(2,1)}, u32[]{:S(2)}) copy-start(bf16[128,256]{1,0:T(8,128)(2,1)} %param.23) | copy-start | bytes 196612
  4.1 21.9 %all-to-all-start.1 = ((bf16[1,16,128]{2,0,1:T(2,128)(2,1)}), bf16[1,16,128]{2,0,1:T(2,128)(2,1)S(1)}, u32[]{:S(2)}, u32[]{:S(2)}) async-start(bf16[1,16,128]{2,0,1:T(2,128)(2,1)} %convert_bitcast_fusion.3), calls=%async_computation.1 | async-start | bytes 16384 | tf_op jit(solution)/shard_map/all_to_all | solution.py:78
  13.5 102.5 %copy-start.10 = (f32[512]{0:T(512)S(1)}, f32[512]{0:T(512)}, u32[]{:S(2)}) copy-start(f32[512]{0:T(512)} %param.31) | copy-start | bytes 6148
  25.4 149.8 %copy-start.8 = (f32[2048]{0:T(1024)S(1)}, f32[2048]{0:T(1024)}, u32[]{:S(2)}) copy-start(f32[2048]{0:T(1024)} %param.33) | copy-start | bytes 24580
  25.4 149.8 %copy-start.2 = (bf16[2048,256]{1,0:T(8,128)(2,1)S(1)}, bf16[2048,256]{1,0:T(8,128)(2,1)}, u32[]{:S(2)}) copy-start(bf16[2048,256]{1,0:T(8,128)(2,1)} %param.39) | copy-start | bytes 3145732
  26.1 133.0 %all-to-all-start = ((bf16[1,16,128]{2,0,1:T(2,128)(2,1)}), bf16[1,16,128]{2,0,1:T(2,128)(2,1)S(1)}, u32[]{:S(2)}, u32[]{:S(2)}) async-start(bf16[1,16,128]{2,0,1:T(2,128)(2,1)} %bitcast), calls=%async_computation | async-start | bytes 16384 | tf_op jit(solution)/shard_map/all_to_all | solution.py:77
  33.5 142.0 %copy-start.3 = (bf16[2048,256]{1,0:T(8,128)(2,1)S(1)}, bf16[2048,256]{1,0:T(8,128)(2,1)}, u32[]{:S(2)}) copy-start(bf16[2048,256]{1,0:T(8,128)(2,1)} %param.40) | copy-start | bytes 3145732
  113.6 0.8 copy-start.1
  159.7 10.7 %all-to-all-start.4 = ((bf16[16,1,128]{2,1,0:T(2,128)(2,1)}), bf16[16,1,128]{2,1,0:T(2,128)(2,1)S(1)}, u32[]{:S(2)}, u32[]{:S(2)}) async-start(bf16[16,1,128]{2,1,0:T(2,128)(2,1)} %copy.73), calls=%async_computation.4 | async-start | bytes 16384 | tf_op jit(solution)/shard_map/all_to_all | solution.py:146
  170.4 11.0 %all-to-all-start.2 = ((bf16[16,12,128]{2,1,0:T(8,128)(2,1)}), bf16[16,12,128]{2,1,0:T(8,128)(2,1)S(1)}, u32[]{:S(2)}, u32[]{:S(2)}) async-start(bf16[16,12,128]{2,1,0:T(8,128)(2,1)} %reshape.471), calls=%async_computation.2 | async-start | bytes 131072 | tf_op jit(solution)/shard_map/all_to_all | solution.py:145
  175.8 18.9 %copy-start.9 = (f32[16,6]{0,1:T(8,128)S(1)}, f32[16,6]{0,1:T(8,128)}, u32[]{:S(2)}) copy-start(f32[16,6]{0,1:T(8,128)} %param.35) | copy-start | bytes 1156
  190.8 28.6 %all-to-all-start.5 = ((bf16[1,1,2048]{1,0,2:T(2,128)(2,1)}), bf16[1,1,2048]{1,0,2:T(2,128)(2,1)S(1)}, u32[]{:S(2)}, u32[]{:S(2)}) async-start(bf16[1,1,2048]{1,0,2:T(2,128)(2,1)} %copy.74), calls=%async_computation.5 | async-start | bytes 2097152 | tf_op jit(solution)/shard_map/all_to_all | solution.py:166
  219.3 22.0 %all-to-all-start.3 = ((bf16[16,2,768]{2,1,0:T(2,128)(2,1)}), bf16[16,2,768]{2,1,0:T(2,128)(2,1)S(1)}, u32[]{:S(2)}, u32[]{:S(2)}) async-start(bf16[16,2,768]{2,1,0:T(2,128)(2,1)} %reshape.519), calls=%async_computation.3 | async-start | bytes 98304 | tf_op jit(solution)/shard_map/all_to_all | solution.py:165
where the time goes:
time: 246 us; the launch traced here: 245 us
  blocking collectives  118 us (48%)
  other arithmetic  34.9 us (14%)
  starting transfers between devices  32.8 us (13%)
  local copies, waits for them, and re-layouts  19.3 us (8%)
  waiting for transfers between devices  18.4 us (7%)
  matrix products  18 us (7%)
  between operations  3.2 us (1%)
    unnamed x1, blocking collectives  78.2 us
    all_gather x1, blocking collectives, per_device(): shard_rows = lax.all_gather(mixed_heads, ('ep', 'tp'), axis=0, tiled=True)  36.5 us
    convert_element_type x1, other arithmetic, per_device(): back_shared.reshape(all_rows, -1).astype(jnp.float32)  15.2 us
    unnamed x1, other arithmetic  12.4 us
    all_to_all x1, waiting for transfers between devices, per_device(): lax.all_to_all(shared_out, 'ep', split_axis=2, concat_axis=0, tiled=True)  8.46 us
    all_to_all x1, starting transfers between devices, per_device(): lax.all_to_all(normed, 'ep', split_axis=1, concat_axis=0, tiled=True)  8.34 us
    all_to_all x1, starting transfers between devices, per_device(): lax.all_to_all(tokens, 'ep', split_axis=1, concat_axis=0, tiled=True)  6.91 us
    all_to_all x1, starting transfers between devices, per_device(): lax.all_to_all(routed_out, 'ep', split_axis=2, concat_axis=0, tiled=True)  6.75 us
  transfers between devices with their start and end apart: 6, of which 3 were waited for; matrix products, arithmetic and copies ran while one was open for 24% of the time, Pallas kernels for 0%

commit v1 on v0

--- a/solution.py
+++ b/solution.py
@@ -1,6 +1,10 @@
+import functools
+
 import jax
 import jax.numpy as jnp
 from jax import lax
+from jax.experimental import pallas as pl
+from jax.experimental.pallas import tpu as pltpu
 from jax.sharding import PartitionSpec as P
 
 DK = 256
@@ -172,9 +176,384 @@
     return (result, new_state)
 
 
+HBM = pltpu.MemorySpace.HBM
+MESH = pl.DeviceIdType.MESH
+
+
+def silu(values):
+    return values / (1.0 + jnp.exp(-values))
+
+
+def rounded(values):
+    return values.astype(jnp.bfloat16).astype(jnp.float32)
+
+
+def layer_kernel(
+    ep_size,
+    tp_size,
+    tokens,
+    norm_gain,
+    w_query,
+    w_key,
+    w_value,
+    w_outgate,
+    decay_in,
+    decay_out,
+    decay_bias,
+    gla_state,
+    head_gain,
+    w_output,
+    moe_gain,
+    expert_ids,
+    route_weight,
+    expert_gate,
+    expert_up,
+    expert_down,
+    shared_gate,
+    shared_up,
+    shared_down,
+    result,
+    new_state,
+    tok_v,
+    gain_v,
+    proj_v,
+    din_v,
+    dout_v,
+    bias_v,
+    state_v,
+    hgain_v,
+    wout_v,
+    mgain_v,
+    ids_v,
+    route_v,
+    up_v,
+    down_v,
+    send_a,
+    recv_a,
+    send_b,
+    recv_b,
+    send_c,
+    recv_c,
+    send_d,
+    recv_d,
+    send_e,
+    recv_e,
+    result_v,
+    local_sem,
+    send_sem,
+    recv_sem,
+):
+    me = lax.axis_index("ep")
+    core = lax.axis_index("tp")
+    devices = ep_size * tp_size
+    flat = me * tp_size + core
+    block = result_v.shape[1]
+    hidden_units = expert_gate.shape[2]
+    shared_units = (up_v.shape[1] - 2 * hidden_units) // 2
+    shared_blocks = shared_gate.shape[1] // shared_units
+    shared_at = pl.multiple_of(lax.rem(me, shared_blocks) * shared_units, shared_units)
+    edges = [0]
+    for weight in (w_query, w_key, w_value, w_outgate):
+        edges.append(edges[-1] + weight.shape[1])
+
+    pending = {}
+
+    def fetch(name, source, target):
+        copy = pltpu.make_async_copy(source, target, local_sem.at[len(pending)])
+        copy.start()
+        pending[name] = copy
+
+    fetch("tokens", tokens, tok_v)
+    fetch("norm_gain", norm_gain, gain_v)
+    for number, weight in enumerate((w_query, w_key, w_value, w_outgate)):
+        fetch(f"proj{number}", weight, proj_v.at[:, pl.ds(edges[number], weight.shape[1])])
+    fetch("decay_in", decay_in, din_v)
+    fetch("decay_out", decay_out, dout_v)
+    fetch("decay_bias", decay_bias, bias_v)
+    fetch("state", gla_state.at[0, 0], state_v)
+    fetch("head_gain", head_gain, hgain_v)
+    fetch("w_output", w_output, wout_v)
+    fetch("moe_gain", moe_gain, mgain_v)
+    fetch("ids", expert_ids, ids_v)
+    fetch("route", route_weight, route_v)
+    fetch("gate", expert_gate.at[0], up_v.at[:, pl.ds(0, hidden_units)])
+    fetch("up", expert_up.at[0], up_v.at[:, pl.ds(hidden_units, hidden_units)])
+    fetch(
+        "sgate",
+        shared_gate.at[:, pl.ds(shared_at, shared_units)],
+        up_v.at[:, pl.ds(2 * hidden_units, shared_units)],
+    )
+    fetch(
+        "sup",
+        shared_up.at[:, pl.ds(shared_at, shared_units)],
+        up_v.at[:, pl.ds(2 * hidden_units + shared_units, shared_units)],
+    )
+    fetch("down", expert_down.at[0], down_v.at[pl.ds(0, hidden_units)])
+    fetch(
+        "sdown",
+        shared_down.at[pl.ds(shared_at, shared_units)],
+        down_v.at[pl.ds(hidden_units, shared_units)],
+    )
+
+    barrier = pltpu.get_barrier_semaphore()
+
+    def to_all(body):
+        def step(number, carry):
+            other = lax.rem(flat + number, devices)
+            body(lax.div(other, tp_size), lax.rem(other, tp_size))
+            return carry
+
+        lax.fori_loop(1, devices, step, 0)
+
+    def to_peers(body):
+        def step(number, carry):
+            body(lax.rem(me + number, ep_size))
+            return carry
+
+        lax.fori_loop(1, ep_size, step, 0)
+
+    def remote(source, target, phase, where):
+        pltpu.make_async_remote_copy(
+            src_ref=source,
+            dst_ref=target,
+            send_sem=send_sem.at[phase],
+            recv_sem=recv_sem.at[phase],
+            device_id=where,
+            device_id_type=MESH,
+        ).start()
+
+    def arrived(span, phase):
+        pltpu.make_async_copy(span, span, recv_sem.at[phase]).wait()
+
+    def left(span, phase):
+        pltpu.make_async_copy(span, span, send_sem.at[phase]).wait()
+
+    def columns(index):
+        return pl.ds(pl.multiple_of(index * block, block), block)
+
+    to_all(lambda e, t: pl.semaphore_signal(barrier, inc=1, device_id=(e, t), device_id_type=MESH))
+
+    pending["tokens"].wait()
+    pending["norm_gain"].wait()
+    raw = tok_v[...].astype(jnp.float32)
+    scale = lax.rsqrt(jnp.mean(raw * raw, axis=-1, keepdims=True) + EPSILON)
+    normed = (raw * scale * gain_v[...]).astype(jnp.bfloat16)
+    send_a[0:1, :] = normed.astype(jnp.float32)
+    send_a[1:2, :] = raw
+    recv_a[me] = send_a[:, columns(me)]
+    pl.semaphore_wait(barrier, devices - 1)
+    to_peers(lambda e: remote(send_a.at[:, columns(e)], recv_a.at[me], 0, (e, core)))
+
+    for name in ("decay_in", "decay_out", "decay_bias", "state"):
+        pending[name].wait()
+    low = jnp.dot(normed, din_v[...], preferred_element_type=jnp.float32).astype(jnp.bfloat16)
+    pre = jnp.dot(low, dout_v[...], preferred_element_type=jnp.float32) + bias_v[...]
+    log_sigmoid = jnp.minimum(pre, 0.0) - jnp.log(1.0 + jnp.exp(-jnp.abs(pre)))
+    rate = jnp.exp(log_sigmoid / DECAY_TEMPER)
+    rate_column = jnp.broadcast_to(rate, (8, DK)).T[:, 0:1]
+    state_v[...] = rate_column * state_v[...]
+
+    for number in range(4):
+        pending[f"proj{number}"].wait()
+    arrived(recv_a.at[pl.ds(0, ep_size - 1)], 0)
+    partial = jnp.dot(
+        recv_a[:, 0, :].astype(jnp.bfloat16), proj_v[...], preferred_element_type=jnp.float32
+    )
+    send_b[...] = partial.reshape(send_b.shape)
+    recv_b[me] = send_b[me]
+    to_peers(lambda e: remote(send_b.at[e], recv_b.at[me], 1, (e, core)))
+    for name in ("head_gain", "w_output", "moe_gain", "ids", "route"):
+        pending[name].wait()
+    arrived(recv_b.at[pl.ds(0, ep_size - 1)], 1)
+    joined = rounded(jnp.sum(recv_b[...], axis=0))
+    query = joined[:, edges[0] : edges[1]] * DK ** (-0.5)
+    key = joined[:, edges[1] : edges[2]]
+    value = joined[:, edges[2] : edges[3]]
+    gate = joined[:, edges[3] : edges[4]]
+    pair = jnp.concatenate(
+        [jnp.broadcast_to(key, (4, DK)), jnp.broadcast_to(query, (4, DK))], axis=0
+    ).T
+    updated = state_v[...] + pair[:, 0:1] * value
+    state_v[...] = updated
+    read_out = jnp.sum(pair[:, 4:5] * updated, axis=0, keepdims=True)
+    read_scale = lax.rsqrt(jnp.mean(read_out * read_out, axis=-1, keepdims=True) + EPSILON)
+    mixed = rounded(read_out * read_scale * hgain_v[...] * silu(gate))
+    send_c[...] = mixed
+    slot = core * ep_size + me
+    recv_c[slot] = mixed
+    to_all(lambda e, t: remote(send_c, recv_c.at[slot], 2, (e, t)))
+    state_out = pltpu.make_async_copy(state_v, new_state.at[0, 0], local_sem.at[len(pending)])
+    state_out.start()
+
+    arrived(recv_c.at[pl.ds(0, devices - 1)], 2)
+    attention = jnp.zeros((ep_size, block), jnp.float32)
+    for head in range(tp_size):
+        rows = recv_c[head * ep_size : (head + 1) * ep_size, 0, :].astype(jnp.bfloat16)
+        attention = attention + jnp.dot(
+            rows, wout_v[head * DV : (head + 1) * DV], preferred_element_type=jnp.float32
+        )
+    hidden = rounded(recv_a[:, 1, :] + rounded(attention))
+    send_d[...] = hidden.astype(jnp.bfloat16)
+    recv_d[:, columns(me)] = hidden.astype(jnp.bfloat16)
+    to_peers(lambda e: remote(send_d, recv_d.at[:, columns(me)], 3, (e, core)))
+
+    routed = jnp.sum(jnp.where(ids_v[...] == me, route_v[...], 0.0), axis=1, keepdims=True)
+    token = lax.broadcasted_iota(jnp.int32, (ep_size, 1), 0)
+    shared = jnp.where(
+        lax.div(token, shared_blocks) == lax.div(me, shared_blocks), 1.0, 0.0
+    )
+    for name in ("gate", "up", "sgate", "sup", "down", "sdown"):
+        pending[name].wait()
+    arrived(recv_d.at[:, pl.ds(0, (ep_size - 1) * block)], 3)
+    rows = recv_d[...].astype(jnp.float32)
+    row_scale = lax.rsqrt(jnp.mean(rows * rows, axis=-1, keepdims=True) + EPSILON)
+    hnorm = (rows * row_scale * mgain_v[...]).astype(jnp.bfloat16)
+    both = jnp.dot(hnorm, up_v[...], preferred_element_type=jnp.float32)
+    cut = 2 * hidden_units
+    active = silu(both[:, :hidden_units]) * both[:, hidden_units:cut] * routed
+    extra = silu(both[:, cut : cut + shared_units]) * both[:, cut + shared_units :] * shared
+    down = jnp.dot(
+        jnp.concatenate([active, extra], axis=1).astype(jnp.bfloat16),
+        down_v[...],
+        preferred_element_type=jnp.float32,
+    )
+    send_e[...] = down.astype(jnp.bfloat16)
+    recv_e[slot] = send_e[:, columns(me)]
+    to_all(lambda e, t: remote(send_e.at[:, columns(e)], recv_e.at[slot], 4, (e, t)))
+    arrived(recv_e.at[pl.ds(0, devices - 1)], 4)
+    total = jnp.sum(recv_e[...].astype(jnp.float32), axis=0)
+    result_v[...] = (hidden + total).astype(jnp.bfloat16)
+    result_out = pltpu.make_async_copy(result_v, result, local_sem.at[len(pending) + 1])
+    result_out.start()
+
+    left(recv_a.at[pl.ds(0, ep_size - 1)], 0)
+    left(recv_b.at[pl.ds(0, ep_size - 1)], 1)
+    left(recv_c.at[pl.ds(0, devices - 1)], 2)
+    left(recv_d.at[:, pl.ds(0, (ep_size - 1) * block)], 3)
+    left(recv_e.at[pl.ds(0, devices - 1)], 4)
+    state_out.wait()
+    result_out.wait()
+
+
+def fused_device(*args):
+    (
+        tokens,
+        norm_gain,
+        w_query,
+        w_key,
+        w_value,
+        w_outgate,
+        decay_in,
+        decay_out,
+        decay_bias,
+        gla_state,
+        head_gain,
+        w_output,
+        moe_gain,
+        expert_ids,
+        route_weight,
+        expert_gate,
+        expert_up,
+        expert_down,
+        shared_gate,
+        shared_up,
+        shared_down,
+    ) = args
+    ep_size = lax.axis_size("ep")
+    tp_size = lax.axis_size("tp")
+    width = tokens.shape[1]
+    block = w_output.shape[1]
+    span = sum(weight.shape[1] for weight in (w_query, w_key, w_value, w_outgate))
+    devices = ep_size * tp_size
+    hidden_units = expert_gate.shape[2]
+    shared_units = min(128, shared_gate.shape[1])
+    rows = [values.reshape(1, -1) for values in (norm_gain, decay_bias, head_gain, moe_gain)]
+    operands = (
+        tokens,
+        rows[0],
+        w_query,
+        w_key,
+        w_value,
+        w_outgate,
+        decay_in,
+        decay_out,
+        rows[1],
+        gla_state,
+        rows[2],
+        w_output,
+        rows[3],
+        expert_ids,
+        route_weight,
+        expert_gate,
+        expert_up,
+        expert_down,
+        shared_gate,
+        shared_up,
+        shared_down,
+    )
+
+    def held(values):
+        return pltpu.VMEM(values.shape, values.dtype)
+
+    scratch = [
+        held(tokens),
+        held(rows[0]),
+        pltpu.VMEM((block, span), jnp.bfloat16),
+        held(decay_in),
+        held(decay_out),
+        held(rows[1]),
+        pltpu.VMEM(gla_state.shape[2:], jnp.float32),
+        held(rows[2]),
+        held(w_output),
+        held(rows[3]),
+        held(expert_ids),
+        held(route_weight),
+        pltpu.VMEM((width, 2 * (hidden_units + shared_units)), jnp.bfloat16),
+        pltpu.VMEM((hidden_units + shared_units, width), jnp.bfloat16),
+        pltpu.VMEM((2, width), jnp.float32),
+        pltpu.VMEM((ep_size, 2, block), jnp.float32),
+        pltpu.VMEM((ep_size, 1, span), jnp.float32),
+        pltpu.VMEM((ep_size, 1, span), jnp.float32),
+        pltpu.VMEM((1, DV), jnp.float32),
+        pltpu.VMEM((devices, 1, DV), jnp.float32),
+        pltpu.VMEM((ep_size, block), jnp.bfloat16),
+        pltpu.VMEM((ep_size, width), jnp.bfloat16),
+        pltpu.VMEM((ep_size, width), jnp.bfloat16),
+        pltpu.VMEM((devices, ep_size, block), jnp.bfloat16),
+        pltpu.VMEM((ep_size, block), jnp.bfloat16),
+        pltpu.SemaphoreType.DMA((len(operands) + 2,)),
+        pltpu.SemaphoreType.DMA((5,)),
+        pltpu.SemaphoreType.DMA((5,)),
+    ]
+    return pl.pallas_call(
+        functools.partial(layer_kernel, ep_size, tp_size),
+        out_shape=(
+            jax.ShapeDtypeStruct((ep_size, block), jnp.bfloat16),
+            jax.ShapeDtypeStruct(gla_state.shape, jnp.float32),
+        ),
+        in_specs=[pl.BlockSpec(memory_space=HBM)] * len(operands),
+        out_specs=(pl.BlockSpec(memory_space=HBM), pl.BlockSpec(memory_space=HBM)),
+        scratch_shapes=scratch,
+        compiler_params=pltpu.CompilerParams(collective_id=0, has_side_effects=True),
+    )(*operands)
+
+
+def chosen_device(*args):
+    tokens, w_query, w_output, expert_gate = args[0], args[2], args[11], args[15]
+    ep_size = lax.axis_size("ep")
+    fits = (
+        tokens.shape[0] == 1
+        and expert_gate.shape[0] == 1
+        and w_query.shape[1] == DK
+        and w_output.shape[1] % 128 == 0
+        and ep_size % (args[18].shape[1] // min(128, args[18].shape[1])) == 0
+    )
+    return fused_device(*args) if fits else per_device(*args)
+
+
 def solution(mesh):
     return jax.shard_map(
-        per_device,
+        chosen_device,
         mesh=mesh,
         in_specs=(
             P("ep", None),

time: 246 us -> 39.4 us (0.16)
  blocking collectives: 118 us -> 0 us
  other arithmetic: 34.9 us -> 0 us
  starting transfers between devices: 32.8 us -> 0 us
  Pallas kernels: 0 us -> 31.4 us
  waiting for transfers between devices: 18.4 us -> 0 us
  matrix products: 18 us -> 0 us
  local copies, waits for them, and re-layouts: 19.3 us -> 7.02 us
  between operations: 3.2 us -> 0.65 us
    unnamed x1 -> x0, blocking collectives: 78.2 us -> none
    all_gather x1 -> x0, blocking collectives: 36.5 us -> none  [per_device(): shard_rows = lax.all_gather(mixed_heads, ('ep', 'tp'), axis=0, tiled=True)]
    all_to_all x6 -> x0, starting transfers between devices: 32.8 us -> none  [the longest x1 8.34 us: per_device(): lax.all_to_all(normed, 'ep', split_axis=1, concat_axis=0, tiled=True)]
    pallas_call x0 -> x1, Pallas kernels: none -> 31.4 us  [fused_device(): pl.pallas_call(functools.partial(layer_kernel, ep_size, tp_size), out_sha...]
    all_to_all x6 -> x0, waiting for transfers between devices: 18.4 us -> none  [the longest x1 8.46 us: per_device(): lax.all_to_all(shared_out, 'ep', split_axis=2, concat_axis=0, tiled=True)]
    dot_general x13 -> x0, matrix products: 18 us -> none  [the longest x1 6.42 us: per_device(): jnp.einsum('msc,mcd->msd', shard_rows, chosen, preferred_element_type=jnp...]
    convert_element_type x11 -> x0, other arithmetic: 16.1 us -> none  [the longest x1 15.2 us: per_device(): back_shared.reshape(all_rows, -1).astype(jnp.float32)]
    unnamed x1 -> x0, other arithmetic: 12.4 us -> none
  transfers between devices with their start and end apart: 6 -> 0, of which waited for: 3 -> 0; matrix products, arithmetic and copies ran while one was open for 24% -> 0% of each run, Pallas kernels for 0% -> 0%
where the time goes in v1:
time: 39.4 us; the launch traced here: 39.1 us
  Pallas kernels  31.4 us (80%)
  local copies, waits for them, and re-layouts  7.02 us (18%)
  between operations  0.65 us (2%)
    pallas_call x1, Pallas kernels, fused_device(): pl.pallas_call(functools.partial(layer_kernel, ep_size, tp_size), out_sha...  31.4 us
    unnamed x9, local copies, waits for them, and re-layouts  7.02 us

profile of v1, /device:TPU:0, one launch (start us, length us, event | category | flops | bytes accessed | tf_op | source)
XLA Modules:
  0.0 39.1 jit_solution(11376609796441403560)
XLA Ops:
  0.6 0.0 copy-start
  0.6 0.7 %copy-done = s32[16,6]{0,1:T(8,128)S(1)} copy-done((s32[16,6]{0,1:T(8,128)S(1)}, s32[16,6]{0,1:T(8,128)}, u32[]{:S(2)}) %copy-start) | copy-done | bytes 408
  1.3 0.0 copy-start.1
  1.3 0.7 %copy.24.expert_ids = s32[16,6]{1,0:T(8,128)} copy(s32[16,6]{0,1:T(8,128)S(1)} %copy-done) | data formatting | bytes 768 | tf_op args[13]
  2.0 0.0 copy-done.1
  2.0 0.7 %copy.25.route_weight = f32[16,6]{1,0:T(8,128)} copy(f32[16,6]{0,1:T(8,128)S(1)} %copy-done.1) | data formatting | bytes 768 | tf_op args[14]
  2.7 1.8 %copy.23.decay_in = bf16[2048,16]{1,0:T(8,128)(2,1)} copy(bf16[2048,16]{0,1:T(8,128)(2,1)} %param.27) | data formatting | bytes 131072 | tf_op args[6]
  4.5 31.4 %shard_map.212 = (bf16[16,128]{1,0:T(8,128)(2,1)}, f32[1,1,256,512]{3,2,1,0:T(8,128)}) custom-call(bf16[1,2048]{1,0:T(2,128)(2,1)} %tokens.1, f32[1,2048]{1,0:T(1,128)} %bitcast.4, bf16[128,256]{1,0:T(8,128)(2,1)} %w_query.1, bf16[128,256]{1,0:T(8,128)(2,1)} %w_key.1, bf16[128,512]{1,0:T(8,128)(2,1)} %w_value.1, bf16[128,512]{1,0:T(8,128)(2,1)} %w_outgate.1, ...), custom_call_target="tpu_custom_call" | custom-call | tf_op jit(solution)/shard_map/pallas_call | solution.py:528
  36.0 1.3 %copy.28 = bf16[16,128]{1,0:T(8,128)(2,1)} copy(bf16[16,128]{1,0:T(8,128)(2,1)} %get-tuple-element.4) | data formatting | bytes 8192
  37.2 1.9 %copy.29 = f32[1,1,256,512]{3,2,1,0:T(8,128)} copy(f32[1,1,256,512]{3,2,1,0:T(8,128)} %get-tuple-element.5) | data formatting | bytes 1048576
Async XLA Ops:
  0.6 0.7 %copy-start = (s32[16,6]{0,1:T(8,128)S(1)}, s32[16,6]{0,1:T(8,128)}, u32[]{:S(2)}) copy-start(s32[16,6]{0,1:T(8,128)} %param.34) | copy-start | bytes 1156
  1.3 0.7 %copy-start.1 = (f32[16,6]{0,1:T(8,128)S(1)}, f32[16,6]{0,1:T(8,128)}, u32[]{:S(2)}) copy-start(f32[16,6]{0,1:T(8,128)} %param.35) | copy-start | bytes 1156

commit v2 on v1

--- a/solution.py
+++ b/solution.py
@@ -220,7 +220,6 @@
     din_v,
     dout_v,
     bias_v,
-    state_v,
     hgain_v,
     wout_v,
     mgain_v,
@@ -238,7 +237,6 @@
     recv_d,
     send_e,
     recv_e,
-    result_v,
     local_sem,
     send_sem,
     recv_sem,
@@ -247,7 +245,8 @@
     core = lax.axis_index("tp")
     devices = ep_size * tp_size
     flat = me * tp_size + core
-    block = result_v.shape[1]
+    block = result.shape[1]
+    state_v = new_state.at[0, 0]
     hidden_units = expert_gate.shape[2]
     shared_units = (up_v.shape[1] - 2 * hidden_units) // 2
     shared_blocks = shared_gate.shape[1] // shared_units
@@ -262,6 +261,42 @@
         copy = pltpu.make_async_copy(source, target, local_sem.at[len(pending)])
         copy.start()
         pending[name] = copy
+
+    barrier = pltpu.get_barrier_semaphore()
+
+    def wrapped(index, size):
+        return jnp.where(index >= size, index - size, index)
+
+    def to_all(body):
+        for step in range(ep_size):
+            for other in range(tp_size):
+                if step or other:
+                    body(wrapped(me + step, ep_size), wrapped(core + other, tp_size))
+
+    def to_peers(body):
+        for step in range(1, ep_size):
+            body(wrapped(me + step, ep_size))
+
+    def remote(source, target, phase, where):
+        pltpu.make_async_remote_copy(
+            src_ref=source,
+            dst_ref=target,
+            send_sem=send_sem.at[phase],
+            recv_sem=recv_sem.at[phase],
+            device_id=where,
+            device_id_type=MESH,
+        ).start()
+
+    def arrived(span, phase):
+        pltpu.make_async_copy(span, span, recv_sem.at[phase]).wait()
+
+    def left(span, phase):
+        pltpu.make_async_copy(span, span, send_sem.at[phase]).wait()
+
+    def columns(index):
+        return pl.ds(pl.multiple_of(index * block, block), block)
+
+    to_all(lambda e, t: pl.semaphore_signal(barrier, inc=1, device_id=(e, t), device_id_type=MESH))
 
     fetch("tokens", tokens, tok_v)
     fetch("norm_gain", norm_gain, gain_v)
@@ -271,6 +306,18 @@
     fetch("decay_out", decay_out, dout_v)
     fetch("decay_bias", decay_bias, bias_v)
     fetch("state", gla_state.at[0, 0], state_v)
+
+    pending["tokens"].wait()
+    pending["norm_gain"].wait()
+    raw = tok_v[...].astype(jnp.float32)
+    scale = lax.rsqrt(jnp.mean(raw * raw, axis=-1, keepdims=True) + EPSILON)
+    normed = (raw * scale * gain_v[...]).astype(jnp.bfloat16)
+    send_a[0:1, :] = normed.astype(jnp.float32)
+    send_a[1:2, :] = raw
+    recv_a[me] = send_a[:, columns(me)]
+    pl.semaphore_wait(barrier, devices - 1)
+    to_peers(lambda e: remote(send_a.at[:, columns(e)], recv_a.at[me], 0, (e, core)))
+
     fetch("head_gain", head_gain, hgain_v)
     fetch("w_output", w_output, wout_v)
     fetch("moe_gain", moe_gain, mgain_v)
@@ -295,58 +342,11 @@
         down_v.at[pl.ds(hidden_units, shared_units)],
     )
 
-    barrier = pltpu.get_barrier_semaphore()
-
-    def to_all(body):
-        def step(number, carry):
-            other = lax.rem(flat + number, devices)
-            body(lax.div(other, tp_size), lax.rem(other, tp_size))
-            return carry
-
-        lax.fori_loop(1, devices, step, 0)
-
-    def to_peers(body):
-        def step(number, carry):
-            body(lax.rem(me + number, ep_size))
-            return carry
-
-        lax.fori_loop(1, ep_size, step, 0)
-
-    def remote(source, target, phase, where):
-        pltpu.make_async_remote_copy(
-            src_ref=source,
-            dst_ref=target,
-            send_sem=send_sem.at[phase],
-            recv_sem=recv_sem.at[phase],
-            device_id=where,
-            device_id_type=MESH,
-        ).start()
-
-    def arrived(span, phase):
-        pltpu.make_async_copy(span, span, recv_sem.at[phase]).wait()
-
-    def left(span, phase):
-        pltpu.make_async_copy(span, span, send_sem.at[phase]).wait()
-
-    def columns(index):
-        return pl.ds(pl.multiple_of(index * block, block), block)
-
-    to_all(lambda e, t: pl.semaphore_signal(barrier, inc=1, device_id=(e, t), device_id_type=MESH))
-
-    pending["tokens"].wait()
-    pending["norm_gain"].wait()
-    raw = tok_v[...].astype(jnp.float32)
-    scale = lax.rsqrt(jnp.mean(raw * raw, axis=-1, keepdims=True) + EPSILON)
-    normed = (raw * scale * gain_v[...]).astype(jnp.bfloat16)
-    send_a[0:1, :] = normed.astype(jnp.float32)
-    send_a[1:2, :] = raw
-    recv_a[me] = send_a[:, columns(me)]
-    pl.semaphore_wait(barrier, devices - 1)
-    to_peers(lambda e: remote(send_a.at[:, columns(e)], recv_a.at[me], 0, (e, core)))
-
     for name in ("decay_in", "decay_out", "decay_bias", "state"):
         pending[name].wait()
-    low = jnp.dot(normed, din_v[...], preferred_element_type=jnp.float32).astype(jnp.bfloat16)
+    low = lax.dot_general(
+        normed, din_v[...], (((1,), (1,)), ((), ())), preferred_element_type=jnp.float32
+    ).astype(jnp.bfloat16)
     pre = jnp.dot(low, dout_v[...], preferred_element_type=jnp.float32) + bias_v[...]
     log_sigmoid = jnp.minimum(pre, 0.0) - jnp.log(1.0 + jnp.exp(-jnp.abs(pre)))
     rate = jnp.exp(log_sigmoid / DECAY_TEMPER)
@@ -359,13 +359,20 @@
     partial = jnp.dot(
         recv_a[:, 0, :].astype(jnp.bfloat16), proj_v[...], preferred_element_type=jnp.float32
     )
-    send_b[...] = partial.reshape(send_b.shape)
+    lanes = send_b.shape[2]
+    for number in range(send_b.shape[1]):
+        send_b[:, number, :] = partial[:, number * lanes : (number + 1) * lanes].astype(
+            jnp.bfloat16
+        )
     recv_b[me] = send_b[me]
     to_peers(lambda e: remote(send_b.at[e], recv_b.at[me], 1, (e, core)))
     for name in ("head_gain", "w_output", "moe_gain", "ids", "route"):
         pending[name].wait()
     arrived(recv_b.at[pl.ds(0, ep_size - 1)], 1)
-    joined = rounded(jnp.sum(recv_b[...], axis=0))
+    summed = rounded(jnp.sum(recv_b[...].astype(jnp.float32), axis=0))
+    joined = jnp.concatenate(
+        [summed[number : number + 1] for number in range(summed.shape[0])], axis=1
+    )
     query = joined[:, edges[0] : edges[1]] * DK ** (-0.5)
     key = joined[:, edges[1] : edges[2]]
     value = joined[:, edges[2] : edges[3]]
@@ -378,17 +385,21 @@
     read_out = jnp.sum(pair[:, 4:5] * updated, axis=0, keepdims=True)
     read_scale = lax.rsqrt(jnp.mean(read_out * read_out, axis=-1, keepdims=True) + EPSILON)
     mixed = rounded(read_out * read_scale * hgain_v[...] * silu(gate))
-    send_c[...] = mixed
+    packed = jnp.concatenate(
+        [mixed[:, part * lanes : (part + 1) * lanes] for part in range(send_c.shape[0])], axis=0
+    ).astype(jnp.bfloat16)
+    send_c[...] = packed
     slot = core * ep_size + me
-    recv_c[slot] = mixed
+    recv_c[slot] = packed
     to_all(lambda e, t: remote(send_c, recv_c.at[slot], 2, (e, t)))
-    state_out = pltpu.make_async_copy(state_v, new_state.at[0, 0], local_sem.at[len(pending)])
-    state_out.start()
 
     arrived(recv_c.at[pl.ds(0, devices - 1)], 2)
     attention = jnp.zeros((ep_size, block), jnp.float32)
     for head in range(tp_size):
-        rows = recv_c[head * ep_size : (head + 1) * ep_size, 0, :].astype(jnp.bfloat16)
+        heads = recv_c[head * ep_size : (head + 1) * ep_size].astype(jnp.float32)
+        rows = jnp.concatenate(
+            [heads[:, part, :] for part in range(send_c.shape[0])], axis=1
+        ).astype(jnp.bfloat16)
         attention = attention + jnp.dot(
             rows, wout_v[head * DV : (head + 1) * DV], preferred_element_type=jnp.float32
         )
@@ -397,7 +408,12 @@
     recv_d[:, columns(me)] = hidden.astype(jnp.bfloat16)
     to_peers(lambda e: remote(send_d, recv_d.at[:, columns(me)], 3, (e, core)))
 
-    routed = jnp.sum(jnp.where(ids_v[...] == me, route_v[...], 0.0), axis=1, keepdims=True)
+    chosen = jnp.sum(jnp.where(ids_v[...] == me, route_v[...], 0.0), axis=0, keepdims=True)
+    square = (ep_size, ep_size)
+    diagonal = lax.broadcasted_iota(jnp.int32, square, 0) == lax.broadcasted_iota(
+        jnp.int32, square, 1
+    )
+    routed = jnp.sum(jnp.where(diagonal, chosen, 0.0), axis=1, keepdims=True)
     token = lax.broadcasted_iota(jnp.int32, (ep_size, 1), 0)
     shared = jnp.where(
         lax.div(token, shared_blocks) == lax.div(me, shared_blocks), 1.0, 0.0
@@ -422,17 +438,24 @@
     to_all(lambda e, t: remote(send_e.at[:, columns(e)], recv_e.at[slot], 4, (e, t)))
     arrived(recv_e.at[pl.ds(0, devices - 1)], 4)
     total = jnp.sum(recv_e[...].astype(jnp.float32), axis=0)
-    result_v[...] = (hidden + total).astype(jnp.bfloat16)
-    result_out = pltpu.make_async_copy(result_v, result, local_sem.at[len(pending) + 1])
-    result_out.start()
+    result[...] = (hidden + total).astype(jnp.bfloat16)
 
     left(recv_a.at[pl.ds(0, ep_size - 1)], 0)
     left(recv_b.at[pl.ds(0, ep_size - 1)], 1)
     left(recv_c.at[pl.ds(0, devices - 1)], 2)
     left(recv_d.at[:, pl.ds(0, (ep_size - 1) * block)], 3)
     left(recv_e.at[pl.ds(0, devices - 1)], 4)
-    state_out.wait()
-    result_out.wait()
+
+
+def write_kernel(result, state, result_out, state_out, sems):
+    copies = [
+        pltpu.make_async_copy(state, state_out, sems.at[0]),
+        pltpu.make_async_copy(result, result_out, sems.at[1]),
+    ]
+    for copy in copies:
+        copy.start()
+    for copy in copies:
+        copy.wait()
 
 
 def fused_device(*args):
@@ -475,15 +498,15 @@
         w_key,
         w_value,
         w_outgate,
-        decay_in,
+        decay_in.T,
         decay_out,
         rows[1],
         gla_state,
         rows[2],
         w_output,
         rows[3],
-        expert_ids,
-        route_weight,
+        expert_ids.T,
+        route_weight.T,
         expert_gate,
         expert_up,
         expert_down,
@@ -499,43 +522,54 @@
         held(tokens),
         held(rows[0]),
         pltpu.VMEM((block, span), jnp.bfloat16),
-        held(decay_in),
+        held(operands[6]),
         held(decay_out),
         held(rows[1]),
-        pltpu.VMEM(gla_state.shape[2:], jnp.float32),
         held(rows[2]),
         held(w_output),
         held(rows[3]),
-        held(expert_ids),
-        held(route_weight),
+        held(operands[13]),
+        held(operands[14]),
         pltpu.VMEM((width, 2 * (hidden_units + shared_units)), jnp.bfloat16),
         pltpu.VMEM((hidden_units + shared_units, width), jnp.bfloat16),
         pltpu.VMEM((2, width), jnp.float32),
         pltpu.VMEM((ep_size, 2, block), jnp.float32),
-        pltpu.VMEM((ep_size, 1, span), jnp.float32),
-        pltpu.VMEM((ep_size, 1, span), jnp.float32),
-        pltpu.VMEM((1, DV), jnp.float32),
-        pltpu.VMEM((devices, 1, DV), jnp.float32),
+        pltpu.VMEM((ep_size, span // 128, 128), jnp.bfloat16),
+        pltpu.VMEM((ep_size, span // 128, 128), jnp.bfloat16),
+        pltpu.VMEM((DV // 128, 128), jnp.bfloat16),
+        pltpu.VMEM((devices, DV // 128, 128), jnp.bfloat16),
         pltpu.VMEM((ep_size, block), jnp.bfloat16),
         pltpu.VMEM((ep_size, width), jnp.bfloat16),
         pltpu.VMEM((ep_size, width), jnp.bfloat16),
         pltpu.VMEM((devices, ep_size, block), jnp.bfloat16),
-        pltpu.VMEM((ep_size, block), jnp.bfloat16),
-        pltpu.SemaphoreType.DMA((len(operands) + 2,)),
+        pltpu.SemaphoreType.DMA((len(operands),)),
         pltpu.SemaphoreType.DMA((5,)),
         pltpu.SemaphoreType.DMA((5,)),
     ]
-    return pl.pallas_call(
+    result, new_state = pl.pallas_call(
         functools.partial(layer_kernel, ep_size, tp_size),
         out_shape=(
-            jax.ShapeDtypeStruct((ep_size, block), jnp.bfloat16),
-            jax.ShapeDtypeStruct(gla_state.shape, jnp.float32),
+            pltpu.VMEM((ep_size, block), jnp.bfloat16),
+            pltpu.VMEM(gla_state.shape, jnp.float32),
         ),
         in_specs=[pl.BlockSpec(memory_space=HBM)] * len(operands),
-        out_specs=(pl.BlockSpec(memory_space=HBM), pl.BlockSpec(memory_space=HBM)),
+        out_specs=(pl.BlockSpec(memory_space=pltpu.VMEM),) * 2,
         scratch_shapes=scratch,
-        compiler_params=pltpu.CompilerParams(collective_id=0, has_side_effects=True),
+        compiler_params=pltpu.CompilerParams(
+            collective_id=0, has_side_effects=True
+        ),
     )(*operands)
+    return pl.pallas_call(
+        write_kernel,
+        out_shape=(
+            jax.ShapeDtypeStruct(result.shape, result.dtype),
+            jax.ShapeDtypeStruct(new_state.shape, new_state.dtype),
+        ),
+        in_specs=[pl.BlockSpec(memory_space=pltpu.VMEM)] * 2,
+        out_specs=(pl.BlockSpec(memory_space=HBM),) * 2,
+        scratch_shapes=[pltpu.SemaphoreType.DMA((2,))],
+        compiler_params=pltpu.CompilerParams(vmem_limit_bytes=8 * 1024 * 1024),
+    )(result, new_state)
 
 
 def chosen_device(*args):

time: 39.4 us -> 32.2 us (0.82)
  local copies, waits for them, and re-layouts: 7.02 us -> 0 us
    unnamed x9 -> x0, local copies, waits for them, and re-layouts: 7.02 us -> none
    pallas_call x1, Pallas kernels: 31.4 us -> 30.5 us  [fused_device(): pl.pallas_call(functools.partial(layer_kernel, ep_size, tp_size), out_sha...]
    pallas_call x0 -> x1, Pallas kernels: none -> 0.81 us  [fused_device(): pl.pallas_call(write_kernel, out_shape=(jax.ShapeDtypeStruct(result.shape...]
where the time goes in v2:
time: 32.2 us; the launch traced here: 32 us
  Pallas kernels  31.3 us (97%)
  between operations  0.65 us (2%)
    pallas_call x1, Pallas kernels, fused_device(): pl.pallas_call(functools.partial(layer_kernel, ep_size, tp_size), out_sha...  30.5 us
    pallas_call x1, Pallas kernels, fused_device(): pl.pallas_call(write_kernel, out_shape=(jax.ShapeDtypeStruct(result.shape...  0.81 us

profile of v2, /device:TPU:0, one launch (start us, length us, event | category | flops | bytes accessed | tf_op | source)
XLA Modules:
  0.0 32.0 jit_solution(1812483035780533914)
XLA Ops:
  0.6 30.5 %shard_map.212 = (bf16[16,128]{1,0:T(8,128)(2,1)S(1)}, f32[1,1,256,512]{3,2,1,0:T(8,128)S(1)}) custom-call(bf16[1,2048]{1,0:T(2,128)(2,1)} %tokens.1, f32[1,2048]{1,0:T(1,128)} %bitcast.8, bf16[128,256]{1,0:T(8,128)(2,1)} %w_query.1, bf16[128,256]{1,0:T(8,128)(2,1)} %w_key.1, bf16[128,512]{1,0:T(8,128)(2,1)} %w_value.1, bf16[128,512]{1,0:T(8,128)(2,1)} %w_outgate.1, ...), custom_call_target="tpu_custom_call" | custom-call | tf_op jit(solution)/shard_map/pallas_call | solution.py:549
  31.1 0.8 %shard_map.213 = (bf16[16,128]{1,0:T(8,128)(2,1)}, f32[1,1,256,512]{3,2,1,0:T(8,128)}) custom-call(bf16[16,128]{1,0:T(8,128)(2,1)S(1)} %get-tuple-element.4.result, f32[1,1,256,512]{3,2,1,0:T(8,128)S(1)} %get-tuple-element.5.state), custom_call_target="tpu_custom_call" | custom-call | tf_op jit(solution)/shard_map/pallas_call | solution.py:562

commit v3 on v2

--- a/solution.py
+++ b/solution.py
@@ -237,6 +237,7 @@
     recv_d,
     send_e,
     recv_e,
+    stage,
     local_sem,
     send_sem,
     recv_sem,
@@ -361,9 +362,8 @@
     )
     lanes = send_b.shape[2]
     for number in range(send_b.shape[1]):
-        send_b[:, number, :] = partial[:, number * lanes : (number + 1) * lanes].astype(
-            jnp.bfloat16
-        )
+        stage[:, number, :] = partial[:, number * lanes : (number + 1) * lanes]
+    send_b[...] = stage[...].astype(jnp.bfloat16)
     recv_b[me] = send_b[me]
     to_peers(lambda e: remote(send_b.at[e], recv_b.at[me], 1, (e, core)))
     for name in ("head_gain", "w_output", "moe_gain", "ids", "route"):
@@ -380,9 +380,10 @@
     pair = jnp.concatenate(
         [jnp.broadcast_to(key, (4, DK)), jnp.broadcast_to(query, (4, DK))], axis=0
     ).T
-    updated = state_v[...] + pair[:, 0:1] * value
-    state_v[...] = updated
-    read_out = jnp.sum(pair[:, 4:5] * updated, axis=0, keepdims=True)
+    read_out = (
+        jnp.sum(pair[:, 4:5] * state_v[...], axis=0, keepdims=True)
+        + jnp.sum(query * key, axis=-1, keepdims=True) * value
+    )
     read_scale = lax.rsqrt(jnp.mean(read_out * read_out, axis=-1, keepdims=True) + EPSILON)
     mixed = rounded(read_out * read_scale * hgain_v[...] * silu(gate))
     packed = jnp.concatenate(
@@ -392,6 +393,7 @@
     slot = core * ep_size + me
     recv_c[slot] = packed
     to_all(lambda e, t: remote(send_c, recv_c.at[slot], 2, (e, t)))
+    state_v[...] = state_v[...] + pair[:, 0:1] * value
 
     arrived(recv_c.at[pl.ds(0, devices - 1)], 2)
     attention = jnp.zeros((ep_size, block), jnp.float32)
@@ -423,8 +425,8 @@
     arrived(recv_d.at[:, pl.ds(0, (ep_size - 1) * block)], 3)
     rows = recv_d[...].astype(jnp.float32)
     row_scale = lax.rsqrt(jnp.mean(rows * rows, axis=-1, keepdims=True) + EPSILON)
-    hnorm = (rows * row_scale * mgain_v[...]).astype(jnp.bfloat16)
-    both = jnp.dot(hnorm, up_v[...], preferred_element_type=jnp.float32)
+    gained = (rows * mgain_v[...]).astype(jnp.bfloat16)
+    both = jnp.dot(gained, up_v[...], preferred_element_type=jnp.float32) * row_scale
     cut = 2 * hidden_units
     active = silu(both[:, :hidden_units]) * both[:, hidden_units:cut] * routed
     extra = silu(both[:, cut : cut + shared_units]) * both[:, cut + shared_units :] * shared
@@ -542,6 +544,7 @@
         pltpu.VMEM((ep_size, width), jnp.bfloat16),
         pltpu.VMEM((ep_size, width), jnp.bfloat16),
         pltpu.VMEM((devices, ep_size, block), jnp.bfloat16),
+        pltpu.VMEM((ep_size, span // 128, 128), jnp.float32),
         pltpu.SemaphoreType.DMA((len(operands),)),
         pltpu.SemaphoreType.DMA((5,)),
         pltpu.SemaphoreType.DMA((5,)),

time: 32.2 us -> 32 us (level)
  no operation moved by 1% of the time
where the time goes in v3:
time: 32 us; the launch traced here: 31.8 us
  Pallas kernels  31.2 us (98%)
  between operations  0.65 us (2%)
    pallas_call x1, Pallas kernels, fused_device(): pl.pallas_call(functools.partial(layer_kernel, ep_size, tp_size), out_sha...  30.4 us
    pallas_call x1, Pallas kernels, fused_device(): pl.pallas_call(write_kernel, out_shape=(jax.ShapeDtypeStruct(result.shape...  0.81 us

profile of v3, /device:TPU:0, one launch (start us, length us, event | category | flops | bytes accessed | tf_op | source)
XLA Modules:
  0.0 31.8 jit_solution(17892462229359355669)
XLA Ops:
  0.6 30.4 %shard_map.212 = (bf16[16,128]{1,0:T(8,128)(2,1)S(1)}, f32[1,1,256,512]{3,2,1,0:T(8,128)S(1)}) custom-call(bf16[1,2048]{1,0:T(2,128)(2,1)} %tokens.1, f32[1,2048]{1,0:T(1,128)} %bitcast.8, bf16[128,256]{1,0:T(8,128)(2,1)} %w_query.1, bf16[128,256]{1,0:T(8,128)(2,1)} %w_key.1, bf16[128,512]{1,0:T(8,128)(2,1)} %w_value.1, bf16[128,512]{1,0:T(8,128)(2,1)} %w_outgate.1, ...), custom_call_target="tpu_custom_call" | custom-call | tf_op jit(solution)/shard_map/pallas_call | solution.py:552
  31.0 0.8 %shard_map.213 = (bf16[16,128]{1,0:T(8,128)(2,1)}, f32[1,1,256,512]{3,2,1,0:T(8,128)}) custom-call(bf16[16,128]{1,0:T(8,128)(2,1)S(1)} %get-tuple-element.4.result, f32[1,1,256,512]{3,2,1,0:T(8,128)S(1)} %get-tuple-element.5.state), custom_call_target="tpu_custom_call" | custom-call | tf_op jit(solution)/shard_map/pallas_call | solution.py:565
